TPU v7x, 512 devices: a whole 4x4x16 slice. The times are simulated.
512 devices in a mesh: sp: 32 (over z, core), tp: 16 (over y, x).
Axes of the slice: x: 4, y: 4, z: 16, core: 2. Of those that a mesh axis runs over, the one named last changes fastest.
Arguments:
- receptance: bfloat16 [8192, 4096], P('sp', 'tp'), may hold values from -6 to 6
- key_vectors: bfloat16 [8192, 4096], P('sp', 'tp'), may hold values from -13 to 13
- value_vectors: bfloat16 [8192, 4096], P('sp', 'tp'), may hold values from -6 to 6
- decay_logits: bfloat16 [8192, 4096], P('sp', 'tp'), may hold values from -20 to 2
- rate_logits: bfloat16 [8192, 4096], P('sp', 'tp'), may hold values from -8 to 4
- gate_logits: bfloat16 [8192, 4096], P('sp', 'tp'), may hold values from -6 to 6
- group_gain: float32 [4096], P('tp'), may hold values from 0.1 to 1.9
- residual: bfloat16 [8192, 4096], P('sp', 'tp'), may hold values from -24 to 24
- mixer_out: bfloat16 [4096, 4096], P(None, 'tp'), may hold values from -0.09375 to 0.09375
- norm_gain: float32 [4096], P('tp'), may hold values from 0.1 to 1.9
- expert_ids: int32 [8192, 2], P('sp'), may hold values from 0 to 31, as said below
- route_weight: float32 [8192, 2], P('sp'), may hold values from 0.25 to 1
- expert_gate: bfloat16 [32, 4096, 1024], P('sp', 'tp'), may hold values from -0.09375 to 0.09375
- expert_up: bfloat16 [32, 4096, 1024], P('sp', 'tp'), may hold values from -0.09375 to 0.09375
- expert_down: bfloat16 [32, 1024, 4096], P('sp', None, 'tp'), may hold values from -0.1875 to 0.1875
Outputs:
- updated: bfloat16 [8192, 4096], P('sp', 'tp')
Inputs may be any that keep to these rules, and one draw needn't show every extreme that they name: `expert_ids`: the experts of a row are different and lie in one group of 8 consecutive experts. In the rows of one index of sp (aligned blocks of 256 rows) no expert is named by more than 32 rows, and in every such block some expert is named by exactly 32 rows.
All inputs are finite; a program needn't handle non-finite values.
Results may differ from a plain program's by a relative error of at most 0.013.
Values may be sent and summed in bfloat16 or wider, within the bound.
No kernel may reach another device: no remote copies, remote signals or barrier semaphores. Data moves between devices by JAX's collectives and lax.ppermute only.
A program may use at most 64 MiB of HBM per device.

v0:
```python
import jax
import jax.numpy as jnp
from jax import lax
from jax.sharding import Mesh
from jax.sharding import PartitionSpec as P

D = 4096
HEAD = 64
SPAN = 32
SP = ("sp_0", "sp_1")


EPS_GROUP = 0.00064
EPS_NORM = 1e-06
HIGHEST = lax.Precision.HIGHEST


def neutral_like(shard, identity):
    return jax.tree.map(
        lambda part, zero: jnp.zeros_like(part) + jnp.asarray(zero, part.dtype), shard, identity
    )


def carried_in(shard, axes, combine, identity):
    before = start = neutral_like(shard, identity)
    so_far = shard
    for axis in reversed(axes):
        size, mine = (lax.axis_size(axis), lax.axis_index(axis))
        pieces = jax.tree.map(
            lambda part, kind: lax.all_gather(part.astype(kind), axis),
            so_far,
            (jnp.bfloat16, jnp.bfloat16),
        )
        inside, so_far = (start, start)
        for k in range(size):
            passed = k < mine
            so_far = combine(
                so_far, jax.tree.map(lambda part, own: part[k].astype(own.dtype), pieces, shard)
            )
            inside = jax.tree.map(lambda new, old: jnp.where(passed, new, old), so_far, inside)
        before = combine(inside, before)
    return before


def from_everyone(shard, axis):
    size = lax.axis_size(axis)
    return lax.all_to_all(
        jnp.broadcast_to(shard[None], (size, *shard.shape)), axis, 0, 0, tiled=True
    )


def joined_along(pieces, dim):
    dims = list(pieces.shape[1:])
    dims[dim] *= pieces.shape[0]
    return jnp.moveaxis(pieces, 0, dim).reshape(dims)


def gather_directly(shard, axis, dim):
    pieces = from_everyone(shard, axis)
    return joined_along(pieces, dim)


def of_everyone(shard, axis):
    everything = from_everyone(shard, axis)
    return jnp.sum(everything, axis=0)


def split_up(shard, dim, size):
    before, after = (shard.shape[:dim], shard.shape[dim + 1 :])
    return jnp.moveaxis(shard.reshape(*before, size, -1, *after), dim, 0)


def sent_and_summed(shard, axis, dim):
    size = lax.axis_size(axis)
    pieces = lax.all_to_all(split_up(shard, dim, size), axis, 0, 0, tiled=True)
    return jnp.sum(pieces.astype(jnp.float32), axis=0)


def exact_einsum(pattern, first_op, second_op):
    return jnp.einsum(pattern, first_op, second_op, precision=HIGHEST)


def block_pieces(recept, keyvec, valvec, logdec, unit_key, correction):
    span_len = recept.shape[1]
    cum_in = jnp.cumsum(logdec, axis=1)
    cum_ex = cum_in - logdec
    cum_end = cum_in[:, span_len - 1 :]
    growth = jnp.exp(-cum_in)
    r_scaled = recept * jnp.exp(cum_in)
    u_scaled = unit_key * jnp.exp(cum_ex)
    k_scaled = keyvec * growth
    c_scaled = correction * growth
    row_pos = lax.broadcasted_iota(jnp.int32, (span_len, span_len), 0)
    col_pos = lax.broadcasted_iota(jnp.int32, (span_len, span_len), 1)
    strict = (col_pos < row_pos).astype(jnp.float32)
    causal = (col_pos <= row_pos).astype(jnp.float32)
    key_pull = exact_einsum("bthn,bshn->bhts", u_scaled, k_scaled) * strict
    corr_pull = exact_einsum("bthn,bshn->bhts", u_scaled, c_scaled) * strict
    key_read = exact_einsum("bthn,bshn->bhts", r_scaled, k_scaled) * causal
    corr_read = exact_einsum("bthn,bshn->bhts", r_scaled, c_scaled) * causal
    system = corr_pull + jnp.eye(span_len, dtype=jnp.float32)
    right_local = exact_einsum("bhts,bshn->bhtn", key_pull, valvec)
    right_start = jnp.swapaxes(u_scaled, 1, 2)
    solved = jax.scipy.linalg.solve_triangular(
        system, jnp.concatenate([right_local, right_start], axis=-1), lower=True, unit_diagonal=True
    )
    channels = valvec.shape[-1]
    pulled_local = solved[..., :channels]
    reach_rows = solved[..., channels:]
    read_local = exact_einsum("bhts,bshn->bthn", key_read, valvec) - exact_einsum(
        "bhts,bhsn->bthn", corr_read, pulled_local
    )
    start_rows = r_scaled - exact_einsum("bhts,bhsn->bthn", corr_read, reach_rows)
    tail_decay = jnp.exp(cum_end - cum_in)
    c_tail = correction * tail_decay
    k_tail = keyvec * tail_decay
    keep_end = jnp.exp(cum_end[:, 0])
    block_map = keep_end[..., :, None] * jnp.eye(channels, dtype=jnp.float32) - exact_einsum(
        "bhtj,bthl->bhjl", reach_rows, c_tail
    )
    block_add = exact_einsum("bthi,bthl->bhil", valvec, k_tail) - exact_einsum(
        "bhti,bthl->bhil", pulled_local, c_tail
    )
    return (read_local, start_rows, block_map, block_add)


def time_mix(
    receptance, key_vectors, value_vectors, decay_logits, rate_logits, gate_logits, group_gain
):
    tokens_here, channels = receptance.shape
    heads_here = channels // HEAD
    block_shape = (tokens_here // SPAN, SPAN, heads_here, HEAD)

    def arrange(array):
        return array.astype(jnp.float32).reshape(block_shape)

    recept = arrange(receptance)
    keyvec = arrange(key_vectors)
    valvec = arrange(value_vectors)
    logdec = -jnp.exp(-jax.nn.softplus(-arrange(decay_logits)) - 0.5)
    unit_key = keyvec / jnp.sqrt(1.0 + jnp.sum(keyvec * keyvec, axis=-1, keepdims=True))
    correction = unit_key * jax.nn.sigmoid(arrange(rate_logits))
    read_local, start_rows, block_map, block_add = block_pieces(
        recept, keyvec, valvec, logdec, unit_key, correction
    )
    eye_heads = jnp.broadcast_to(jnp.eye(HEAD, dtype=jnp.float32), (heads_here, HEAD, HEAD))
    zero_heads = jnp.zeros((heads_here, HEAD, HEAD), jnp.float32)

    def advance(carried, inputs):
        local_state, product = carried
        step_map, step_add = inputs
        new_state = exact_einsum("hij,hjl->hil", local_state, step_map) + step_add
        new_product = exact_einsum("hij,hjl->hil", product, step_map)
        return ((new_state, new_product), (local_state, product))

    (device_add, device_map), (starts, products) = lax.scan(
        advance, (zero_heads, eye_heads), (block_map, block_add)
    )

    def compose(earlier, following):
        return (
            exact_einsum("hij,hjl->hil", earlier[0], following[0]),
            exact_einsum("hij,hjl->hil", earlier[1], following[0]) + following[1],
        )

    prefix = carried_in((device_map, device_add), SP, compose, (eye_heads, zero_heads))
    incoming = prefix[1]
    from_local = exact_einsum("bthj,bhij->bthi", start_rows, starts)
    through = exact_einsum("bthl,bhjl->bthj", start_rows, products)
    state_read = read_local + from_local + exact_einsum("bthj,hij->bthi", through, incoming)
    centred = state_read - jnp.mean(state_read, axis=-1, keepdims=True)
    scaled = centred * lax.rsqrt(jnp.mean(centred * centred, axis=-1, keepdims=True) + EPS_GROUP)
    gated_out = (
        scaled.reshape(tokens_here, channels)
        * group_gain[None, :]
        * jax.nn.sigmoid(gate_logits.astype(jnp.float32))
    )
    return gated_out.astype(jnp.bfloat16)


def local(
    receptance,
    key_vectors,
    value_vectors,
    decay_logits,
    rate_logits,
    gate_logits,
    group_gain,
    residual,
    mixer_out,
    norm_gain,
    expert_ids,
    route_weight,
    expert_gate,
    expert_up,
    expert_down,
):
    mixed_rows = time_mix(
        receptance, key_vectors, value_vectors, decay_logits, rate_logits, gate_logits, group_gain
    )
    tokens_here, features = residual.shape
    projected = jnp.dot(
        gather_directly(mixed_rows, "tp", 1), mixer_out, preferred_element_type=jnp.float32
    )
    midway = (residual.astype(jnp.float32) + projected).astype(jnp.bfloat16)
    midway_f = midway.astype(jnp.float32)
    squares = of_everyone(jnp.sum(midway_f * midway_f, axis=1), "tp")
    inv_rms = lax.rsqrt(squares / D + EPS_NORM)
    normed = (midway_f * norm_gain[None, :] * inv_rms[:, None]).astype(jnp.bfloat16)
    routes = expert_ids.shape[1]
    experts_all = lax.axis_size(SP) * expert_gate.shape[0]
    capacity = 2 * tokens_here * routes // experts_all
    flat_ids = expert_ids.reshape(-1)
    onehot = (flat_ids[:, None] == jnp.arange(experts_all, dtype=jnp.int32)[None, :]).astype(
        jnp.int32
    )
    earlier_count = jnp.sum((jnp.cumsum(onehot, axis=0) - onehot) * onehot, axis=1)
    slot_of = flat_ids * capacity + earlier_count
    owner_token = jnp.arange(tokens_here * routes, dtype=jnp.int32) // routes
    slot_table = (
        jnp.full((experts_all * capacity,), tokens_here, jnp.int32).at[slot_of].set(owner_token)
    )
    padded = jnp.concatenate([normed, jnp.zeros((1, features), jnp.bfloat16)], axis=0)
    outgoing = padded[slot_table].reshape(experts_all, capacity, features)
    arrived = lax.all_to_all(outgoing, SP, split_axis=0, concat_axis=0, tiled=True)
    arrived_rows = arrived.reshape(-1, features)
    paired = jnp.concatenate([expert_gate[0], expert_up[0]], axis=1)
    gate_up = sent_and_summed(
        jnp.dot(arrived_rows, paired, preferred_element_type=jnp.float32).astype(jnp.bfloat16),
        "tp",
        0,
    )
    half_width = paired.shape[1] // 2
    hidden = (jax.nn.silu(gate_up[:, :half_width]) * gate_up[:, half_width:]).astype(jnp.bfloat16)
    expert_res = jnp.dot(
        gather_directly(hidden, "tp", 0), expert_down[0], preferred_element_type=jnp.float32
    )
    returned = lax.all_to_all(
        expert_res.astype(jnp.bfloat16).reshape(-1, capacity, features),
        SP,
        split_axis=0,
        concat_axis=0,
        tiled=True,
    )
    picked = (
        returned.reshape(-1, features)[slot_of]
        .astype(jnp.float32)
        .reshape(tokens_here, routes, features)
    )
    routed_sum = jnp.sum(picked * route_weight[:, :, None], axis=1)
    return (midway_f + routed_sum).astype(jnp.bfloat16)


def solution(mesh):
    torus = Mesh(mesh.devices.reshape(16, 2, mesh.shape["tp"]), ("sp_0", "sp_1", "tp"))
    return jax.shard_map(
        local,
        mesh=torus,
        in_specs=(
            P(SP, "tp"),
            P(SP, "tp"),
            P(SP, "tp"),
            P(SP, "tp"),
            P(SP, "tp"),
            P(SP, "tp"),
            P("tp"),
            P(SP, "tp"),
            P(None, "tp"),
            P("tp"),
            P(SP, None),
            P(SP, None),
            P(SP, "tp", None),
            P(SP, "tp", None),
            P(SP, None, "tp"),
        ),
        out_specs=P(SP, "tp"),
        check_vma=False,
    )
```

profile of v0, /device:TPU:1, one launch (start us, length us, event | category | flops | bytes accessed | tf_op | source)
XLA Modules:
  0.0 452.3 jit_solution(2173442664199103637)
XLA Ops:
  0.7 1.0 convert_negate_fusion
  2.0 0.8 copy-done.5
  5.4 0.7 copy.246
  6.3 1.0 div.42
  7.4 1.2 reshape.228
  8.5 1.0 multiply_reduce_fusion.2
  9.5 1.6 copy.206
  11.2 0.7 add_sqrt_fusion
  12.5 2.0 reshape.226
  14.5 1.4 copy.213
  15.9 0.7 copy.214
  16.6 3.0 convolution_multiply_fusion.3
  19.6 1.4 fusion.45
  21.1 1.9 convolution_multiply_fusion
  22.9 1.8 convolution_multiply_fusion.1
  24.8 1.8 fusion.18
  26.6 80.2 %custom-call.4 = f32[8,4,1,32,32]{3,4,2,1,0:T(8,128)} custom-call(f32[8,4,1,32,32]{4,3,2,1,0:T(8,128)} %fusion.18), custom_call_target="InvertDiagBlocksLowerTriangular" | custom-call | tf_op jit(solution)/shard_map/jit(_solve_triangular)/vmap(vmap())/triangular_solve | solution.py:104
  106.8 1.0 convolution_bitcast_fusion.2
  108.7 1.1 fusion.30
  109.9 1.5 fusion.15
  111.4 1.4 fusion.16
  112.8 2.8 convolution_subtract_fusion
  115.6 2.2 convolution_subtract_fusion.1
  117.8 24.8 %while.17 = (s32[]{:T(128)}, f32[4,64,64]{1,2,0:T(8,128)S(1)}, f32[4,64,64]{1,2,0:T(8,128)S(1)}, f32[8,4,64,64]{2,3,1,0:T(8,128)}, f32[8,4,64,64]{2,3,0,1:T(8,12...) while((s32[]{:T(128)}, f32[4,64,64]{1,2,0:T(8,128)S(1)}, ...), condition=%wide.region_3.4_spmd.clone, body=%wide.region_2.3_spmd.clone.sunk | while | flops 25214980 | bytes 1377915 | solution.py:156
  118.5 1.3 fusion.167
  119.8 0.7 bitcast_dynamic-update-slice_fusion.5
  121.6 1.3 fusion.167
  124.7 1.3 fusion.167
  126.0 0.7 bitcast_dynamic-update-slice_fusion.5
  127.8 1.3 fusion.167
  129.1 0.7 bitcast_dynamic-update-slice_fusion.5
  130.9 1.3 fusion.167
  132.2 0.7 bitcast_dynamic-update-slice_fusion.5
  134.0 1.3 fusion.167
  135.3 0.7 bitcast_dynamic-update-slice_fusion.5
  137.1 1.3 fusion.167
  140.2 1.3 fusion.167
  141.5 0.7 bitcast_dynamic-update-slice_fusion.5
  142.7 8.3 %all-gather.2 = bf16[8,64,64]{2,1,0:T(8,128)(2,1)S(1)} all-gather(bf16[4,64,64]{2,1,0:T(8,128)(2,1)S(1)} %copy.223), channel_id=4, replica_groups=mesh['sp_0'=16,'sp_1'=2,'tp'=16] {'sp_1'}, dimensions={0}, use_global_device_ids=true | all-gather | bytes 98304 | tf_op jit(solution)/shard_map/all_gather | solution.py:30
  151.2 1.9 all-gather
  153.9 29.5 %all-gather.1 = bf16[64,64,64]{2,1,0:T(8,128)(2,1)S(1)} all-gather(bf16[4,64,64]{2,1,0:T(8,128)(2,1)S(1)} %get-tuple-element.134), channel_id=3, replica_groups=mesh['sp_0'=16,'sp_1'=2,'tp'=16] {'sp_0'}, dimensions={0}, use_global_device_ids=true | all-gather | bytes 557056 | tf_op jit(solution)/shard_map/all_gather | solution.py:30
  183.4 26.2 %all-gather.3 = bf16[64,64,64]{2,1,0:T(8,128)(2,1)S(1)} all-gather(bf16[4,64,64]{2,1,0:T(8,128)(2,1)S(1)} %get-tuple-element.132), channel_id=5, replica_groups=mesh['sp_0'=16,'sp_1'=2,'tp'=16] {'sp_0'}, dimensions={0}, use_global_device_ids=true | all-gather | bytes 557056 | tf_op jit(solution)/shard_map/all_gather | solution.py:30
  212.6 1.0 convolution_bitcast_fusion.4
  215.4 1.1 fusion.118
  218.2 1.5 broadcast_in_dim.31
  219.7 7.0 %all-to-all-start = ((bf16[16,256,256]{1,2,0:T(8,128)(2,1)}), bf16[16,256,256]{1,2,0:T(8,128)(2,1)}, u32[]{:S(2)}, u32[]{:S(2)}) async-start(bf16[16,256,256]{1,2,0:T(8,128)(2,1)} %broadcast_in_dim.31), calls=%async_computation | async-start | bytes 4194304 | tf_op jit(solution)/shard_map/all_to_all | solution.py:47
  227.5 1.2 reduce-window.6
  229.0 2.4 scatter_custom_fusion
  231.5 15.2 %all-to-all-done = bf16[16,256,256]{1,2,0:T(8,128)(2,1)} async-done(((bf16[16,256,256]{1,2,0:T(8,128)(2,1)}), bf16[16,256,256]{1,2,0:T(8,128)(2,1)}, u32[]{:S(2)}, u32[]{:S(2)}) %all-to-all-start) | async-done | bytes 2097184 | tf_op jit(solution)/shard_map/all_to_all | solution.py:47
  246.7 2.4 multiply_reduce_fusion.3
  249.8 3.5 all-to-all-start.1
  253.3 6.7 %all-to-all-done.1 = f32[16,1,256]{2,1,0:T(1,128)S(1)} async-done(((f32[16,1,256]{2,1,0:T(1,128)}), f32[16,1,256]{2,1,0:T(1,128)S(1)}, u32[]{:S(2)}, u32[]{:S(2)}) %all-to-all-start.1) | async-done | bytes 16416 | tf_op jit(solution)/shard_map/all_to_all | solution.py:47
  260.1 3.9 gather_fusion
  264.1 56.7 %all_to_all.31 = bf16[32,32,256]{2,1,0:T(8,128)(2,1)S(1)} all-to-all(bf16[32,32,256]{2,1,0:T(8,128)(2,1)S(1)} %bitcast.150), channel_id=1, replica_groups=mesh['sp_0'=16,'sp_1'=2,'tp'=16] {'sp_0','sp_1'}, dimensions={0} | all-to-all | bytes 1048576 | tf_op jit(solution)/shard_map/all_to_all | solution.py:225
  320.8 2.3 convolution_convert_fusion
  323.1 52.7 %all_to_all.32 = bf16[16,64,2048]{2,1,0:T(8,128)(2,1)S(1)} all-to-all(bf16[16,64,2048]{2,1,0:T(8,128)(2,1)S(1)} %bitcast.145), channel_id=1, replica_groups=mesh['sp_0'=16,'sp_1'=2,'tp'=16] {'tp'}, dimensions={0} | all-to-all | bytes 8388608 | tf_op jit(solution)/shard_map/all_to_all | solution.py:75
  375.8 0.8 convert_reduce_fusion
  376.9 30.5 %all_to_all.33 = bf16[16,64,1024]{2,1,0:T(8,128)(2,1)S(1)} all-to-all(bf16[16,64,1024]{2,1,0:T(8,128)(2,1)S(1)} %broadcast_in_dim.35), channel_id=1, replica_groups=mesh['sp_0'=16,'sp_1'=2,'tp'=16] {'tp'}, dimensions={0} | all-to-all | bytes 4194304 | tf_op jit(solution)/shard_map/all_to_all | solution.py:47
  407.4 1.5 convolution_convert_fusion.1
  409.0 6.2 %all-to-all-start.5 = ((bf16[32,32,256]{2,1,0:T(8,128)(2,1)}), bf16[32,32,256]{2,1,0:T(8,128)(2,1)S(1)}, u32[]{:S(2)}, u32[]{:S(2)}) async-start(bf16[32,32,256]{2,1,0:T(8,128)(2,1)} %bitcast.24), calls=%async_computation.5 | async-start | bytes 1048576 | tf_op jit(solution)/shard_map/all_to_all | solution.py:238
  415.3 33.4 %all-to-all-done.5 = bf16[32,32,256]{2,1,0:T(8,128)(2,1)S(1)} async-done(((bf16[32,32,256]{2,1,0:T(8,128)(2,1)}), bf16[32,32,256]{2,1,0:T(8,128)(2,1)S(1)}, u32[]{:S(2)}, u32[]{:S(2)}) %all-to-all-start.5) | async-done | bytes 524320 | tf_op jit(solution)/shard_map/all_to_all | solution.py:238
  448.7 1.9 gather_fusion.1
  450.9 0.7 multiply_reduce_fusion
  451.6 0.7 add_convert_fusion
  (186 shorter events, 25.0 us)
Async XLA Ops:
  0.0 246.7 %copy-start = (bf16[4096,256]{1,0:T(8,128)(2,1)S(1)}, bf16[4096,256]{1,0:T(8,128)(2,1)}, u32[]{:S(2)}) copy-start(bf16[4096,256]{1,0:T(8,128)(2,1)} %param.25) | copy-start | bytes 6291460
  0.0 6.1 %copy-start.23 = (bf16[256,256]{1,0:T(8,128)(2,1)S(1)}, bf16[256,256]{1,0:T(8,128)(2,1)}, u32[]{:S(2)}) copy-start(bf16[256,256]{1,0:T(8,128)(2,1)} %param.19) | copy-start | bytes 393220
  0.0 6.2 %copy-start.24 = (bf16[256,256]{1,0:T(8,128)(2,1)S(1)}, bf16[256,256]{1,0:T(8,128)(2,1)}, u32[]{:S(2)}) copy-start(bf16[256,256]{1,0:T(8,128)(2,1)} %param.21) | copy-start | bytes 393220
  0.1 5.3 %copy-start.14 = (f32[64,64]{1,0:T(8,128)}, f32[64,64]{1,0:T(8,128)S(1)}, u32[]{:S(2)}) copy-start(f32[64,64]{1,0:T(8,128)S(1)} %fusion.99) | copy-start | bytes 49156
  1.9 0.8 copy-start.5
  14.5 5.1 %copy-start.6 = (f32[8,32,4,64]{3,2,1,0:T(4,128)S(1)}, f32[8,32,4,64]{3,2,1,0:T(4,128)}, u32[]{:S(2)}) copy-start(f32[8,32,4,64]{3,2,1,0:T(4,128)} %copy-done.5) | copy-start | bytes 786436
  14.5 5.1 %copy-start.11 = (f32[8,32,4,64]{3,2,1,0:T(4,128)S(1)}, f32[8,32,4,64]{3,2,1,0:T(4,128)}, u32[]{:S(2)}) copy-start(f32[8,32,4,64]{3,2,1,0:T(4,128)} %div.42) | copy-start | bytes 786436
  14.5 5.1 %copy-start.30 = (f32[8,32,4]{1,2,0:T(4,128)S(1)}, f32[8,32,4]{1,2,0:T(4,128)}, u32[]{:S(2)}) copy-start(f32[8,32,4]{1,2,0:T(4,128)} %copy.207) | copy-start | bytes 12292
  16.6 4.4 copy-start.21
  19.6 1.5 copy-start.1
  19.6 3.3 copy-start.20
  21.0 3.7 copy-start.3
  21.0 3.7 copy-start.27
  21.0 3.7 copy-start.28
  21.0 3.7 copy-start.31
  22.9 83.8 %copy-start.22 = (f32[8,4,64]{2,1,0:T(4,128)S(1)}, f32[8,4,64]{2,1,0:T(4,128)}, u32[]{:S(2)}) copy-start(f32[8,4,64]{2,1,0:T(4,128)} %copy-done.21) | copy-start | bytes 24580
  106.8 1.1 copy-start.10
  106.8 1.5 copy-start.12
  106.8 1.9 copy-start.4
  106.8 1.9 copy-start.18
  107.8 2.0 copy-start.2
  107.8 2.0 copy-start.9
  109.8 3.0 copy-start.8
  112.8 2.8 copy-start.15
  112.8 2.8 copy-start.29
  112.8 5.0 %copy-start.25 = (f32[64,64]{0,1:T(8,128)S(1)}, f32[64,64]{0,1:T(8,128)}, u32[]{:S(2)}) copy-start(f32[64,64]{0,1:T(8,128)} %copy.246) | copy-start | bytes 49156
  210.4 2.2 copy-start.7
  210.4 2.2 copy-start.17
  213.9 1.4 copy-start.13
  213.9 1.4 copy-start.16
  216.5 1.5 copy-start.26
  216.5 1.5 copy-start.34
  219.7 7.0 %copy-start.32 = (s32[256,2]{0,1:T(2,128)S(1)}, s32[256,2]{0,1:T(2,128)}, u32[]{:S(2)}) copy-start(s32[256,2]{0,1:T(2,128)} %param.27) | copy-start | bytes 6148
  219.7 27.0 %copy-start.37 = (bf16[256,256]{1,0:T(8,128)(2,1)S(1)}, bf16[256,256]{1,0:T(8,128)(2,1)}, u32[]{:S(2)}) copy-start(bf16[256,256]{1,0:T(8,128)(2,1)} %param.24) | copy-start | bytes 393220
  219.7 27.0 %all-to-all-start = ((bf16[16,256,256]{1,2,0:T(8,128)(2,1)}), bf16[16,256,256]{1,2,0:T(8,128)(2,1)}, u32[]{:S(2)}, u32[]{:S(2)}) async-start(bf16[16,256,256]{1,2,0:T(8,128)(2,1)} %broadcast_in_dim.31), calls=%async_computation | async-start | bytes 4194304 | tf_op jit(solution)/shard_map/all_to_all | solution.py:47
  246.7 13.3 %copy-start.35 = (f32[256]{0:T(256)S(1)}, f32[256]{0:T(256)}, u32[]{:S(2)}) copy-start(f32[256]{0:T(256)} %param.26) | copy-start | bytes 3076
  249.8 10.2 %all-to-all-start.1 = ((f32[16,1,256]{2,1,0:T(1,128)}), f32[16,1,256]{2,1,0:T(1,128)S(1)}, u32[]{:S(2)}, u32[]{:S(2)}) async-start(f32[16,1,256]{2,1,0:T(1,128)} %broadcast_in_dim.32), calls=%async_computation.1 | async-start | bytes 32768 | tf_op jit(solution)/shard_map/all_to_all | solution.py:47
  260.1 60.7 %copy-start.19 = (bf16[1,256,1024]{2,1,0:T(8,128)(2,1)S(1)}, bf16[1,256,1024]{2,1,0:T(8,128)(2,1)}, u32[]{:S(2)}) copy-start(bf16[1,256,1024]{2,1,0:T(8,128)(2,1)} %param.30) | copy-start | bytes 1572868
  376.9 30.5 %copy-start.36 = (bf16[1,1024,256]{2,1,0:T(8,128)(2,1)S(1)}, bf16[1,1024,256]{2,1,0:T(8,128)(2,1)}, u32[]{:S(2)}) copy-start(bf16[1,1024,256]{2,1,0:T(8,128)(2,1)} %param.31) | copy-start | bytes 1572868
  407.4 7.7 %copy-start.33 = (f32[256,2]{0,1:T(2,128)S(1)}, f32[256,2]{0,1:T(2,128)}, u32[]{:S(2)}) copy-start(f32[256,2]{0,1:T(2,128)} %param.28) | copy-start | bytes 6148
  409.0 39.7 %all-to-all-start.5 = ((bf16[32,32,256]{2,1,0:T(8,128)(2,1)}), bf16[32,32,256]{2,1,0:T(8,128)(2,1)S(1)}, u32[]{:S(2)}, u32[]{:S(2)}) async-start(bf16[32,32,256]{2,1,0:T(8,128)(2,1)} %bitcast.24), calls=%async_computation.5 | async-start | bytes 1048576 | tf_op jit(solution)/shard_map/all_to_all | solution.py:238
where the time goes:
time: 453 us; the launch traced here: 452 us
  blocking collectives  206 us (45%)
  other arithmetic  96.4 us (21%)
  waiting for transfers between devices  55.2 us (12%)
  matrix products  46.5 us (10%)
  local copies, waits for them, and re-layouts  30.4 us (7%)
  starting transfers between devices  16.6 us (4%)
    another operation x3, other arithmetic, block_pieces(): jax.scipy.linalg.solve_triangular(system, jnp.concatenate([right_local, r...  80.9 us
    all_gather x4, blocking collectives, carried_in(): lax.all_gather(part.astype(kind), axis)  65.9 us
    all_to_all x1, blocking collectives, local(): lax.all_to_all(outgoing, SP, split_axis=0, concat_axis=0, tiled=True)  56.7 us
    all_to_all x1, blocking collectives, sent_and_summed(): pieces = lax.all_to_all(split_up(shard, dim, size), axis, 0, 0, tiled=True)  52.7 us
    dot_general x53, matrix products, exact_einsum(): return jnp.einsum(pattern, first_op, second_op, precision=HIGHEST)  39.1 us
    all_to_all x1, waiting for transfers between devices, local(): lax.all_to_all(expert_res.astype(jnp.bfloat16).reshape(-1, capacity, feat...  33.4 us
    all_to_all x1, blocking collectives, from_everyone(): lax.all_to_all(jnp.broadcast_to(shard[None], (size, *shard.shape)), axis,...  30.5 us
    all_to_all x2, waiting for transfers between devices, from_everyone(): lax.all_to_all(jnp.broadcast_to(shard[None], (size, *shard.shape)), axis,...  21.9 us
  transfers between devices with their start and end apart: 3, of which 3 were waited for; matrix products, arithmetic and copies ran while one was open for 1% of the time, Pallas kernels for 0%

commit v1 on v0

v1 whole, which is shorter than its diff:
```python
import jax
import jax.numpy as jnp
from jax import lax
from jax.experimental import pallas as pl
from jax.experimental.pallas import tpu as pltpu
from jax.sharding import Mesh
from jax.sharding import PartitionSpec as P

D = 4096
SP = ("sp_0", "sp_1")
EPS_NORM = 1e-06
HEAD = 64
SPAN = 64
SUB = 16
LANES = 128
NT = (((1,), (1,)), ((), ()))
NN = (((1,), (0,)), ((), ()))
TN = (((0,), (0,)), ((), ()))
EPS_GROUP = 0.00064
F32 = jnp.float32
BF16 = jnp.bfloat16


def dot(a, b, dims):
    return lax.dot_general(a, b, dims, preferred_element_type=F32)


def split(a):
    high = a.astype(BF16)
    return high, (a - high.astype(F32)).astype(BF16)


def dot_exact(a, b, dims):
    a_high, a_low = split(a)
    b_high, b_low = split(b)
    return dot(a_high, b_high, dims) + (dot(a_high, b_low, dims) + dot(a_low, b_high, dims))


def dot_left(a, b, dims):
    a_high, a_low = split(a)
    return dot(a_high, b, dims) + dot(a_low, b, dims)


def dot_right(a, b, dims):
    b_high, b_low = split(b)
    return dot(a, b_high, dims) + dot(a, b_low, dims)


def iota(shape, dim):
    return lax.broadcasted_iota(jnp.int32, shape, dim)


def head_sums(values):
    width = values.shape[1]
    ones = (iota((width, width), 0) // HEAD == iota((width, width), 1) // HEAD).astype(F32).astype(BF16)
    return dot_left(values, ones, NN)


def paired_diag(pair):
    first = iota(pair.shape, 1) < HEAD
    return jnp.concatenate([jnp.where(first, pair, 0.0), jnp.where(first, 0.0, pair)], axis=0)


def follow(earlier, later):
    carried = dot_exact(earlier, paired_diag(later[HEAD:]), NN)
    return jnp.concatenate([carried[:HEAD] + later[:HEAD], carried[HEAD:]], axis=0)


def state_kernel(r_ref, k_ref, v_ref, d_ref, b_ref, local_ref, start_ref, prefix_ref, total_ref, low_ref, x_ref):
    tokens, width = k_ref.shape
    heads = width // HEAD
    spans = tokens // SPAN
    pairs = heads // 2
    key = k_ref[...].astype(F32)
    recept = r_ref[...].astype(F32)
    unit = key * lax.rsqrt(1.0 + head_sums(key * key))
    corr = unit * jax.nn.sigmoid(b_ref[...].astype(F32))
    logdec = -0.6065306597126334 * jax.nn.sigmoid(d_ref[...].astype(F32))
    lower = (iota((SPAN, SPAN), 1) <= iota((SPAN, SPAN), 0)).astype(F32).astype(BF16)
    lane_head = iota((SPAN, width), 1) // HEAD
    tall = heads * SPAN
    place = iota((tall, LANES), 0) % SPAN
    source = iota((tall, LANES), 1) % SPAN
    first = iota((SPAN, LANES), 1) < HEAD
    reads = []
    kept = []
    for n in range(spans):
        rows = slice(n * SPAN, (n + 1) * SPAN)
        ld = logdec[rows]
        ld_high, ld_rest = split(ld)
        ld_low = (ld - ld_high.astype(F32) - ld_rest.astype(F32)).astype(BF16)
        cum = dot(lower, ld_high, NN) + (dot(lower, ld_rest, NN) + dot(lower, ld_low, NN))
        end = cum[SPAN - 1 :]
        grow = jnp.exp(-cum)
        tail = jnp.exp(end - cum)
        r_in = recept[rows] * jnp.exp(cum)
        u_in = unit[rows] * jnp.exp(cum - ld)
        k_out = key[rows] * grow
        c_out = corr[rows] * grow
        k_tail = key[rows] * tail
        c_tail = corr[rows] * tail
        queries = jnp.concatenate(
            [jnp.where(lane_head == h, q, 0.0) for q in (u_in, r_in) for h in range(heads)], axis=0
        )
        pulls = dot_exact(queries, jnp.concatenate([c_out, k_out], axis=0), NT)
        pull_u = jnp.where(source < place, pulls[:tall], 0.0)
        pull_r = jnp.where(source <= place, pulls[tall:], 0.0)
        value = v_ref[rows, :]
        both = jnp.concatenate([pull_u, pull_r], axis=0)[:, HEAD:]
        by_value = dot_left(both, value, NN)
        low_ref[pl.ds(n * tall, tall), :] = pull_u
        for h in range(heads):
            p = h // 2
            lanes = slice(p * LANES, (p + 1) * LANES)
            kv = by_value[h * SPAN : (h + 1) * SPAN, lanes]
            krv = by_value[tall + h * SPAN : tall + (h + 1) * SPAN, lanes]
            u_tile = u_in[:, lanes]
            r_tile = r_in[:, lanes]
            if h % 2 == 0:
                rhs = jnp.where(first, kv, pltpu.roll(u_tile, HEAD, 1))
                base = jnp.where(first, krv, pltpu.roll(r_tile, HEAD, 1))
            else:
                rhs = jnp.where(first, pltpu.roll(kv, HEAD, 1), u_tile)
                base = jnp.where(first, pltpu.roll(krv, HEAD, 1), r_tile)
            x_ref[pl.ds((n * heads + h) * SPAN, SPAN), :] = rhs
            reads.append((base, pull_r[h * SPAN : (h + 1) * SPAN, :HEAD]))
        kept.append((c_tail, k_tail, end))
    systems = spans * heads
    for b in range(SPAN // SUB):
        if b > 0:
            for s in range(systems):
                at = s * SPAN
                done = x_ref[at : at + b * SUB, :]
                coef = low_ref[at + b * SUB : at + (b + 1) * SUB, : b * SUB]
                x_ref[at + b * SUB : at + (b + 1) * SUB, :] = x_ref[
                    at + b * SUB : at + (b + 1) * SUB, :
                ] - dot_exact(coef, done, NN)
        solved = []
        for t in range(b * SUB, (b + 1) * SUB):
            now = x_ref[pl.ds(t, systems, stride=SPAN), :]
            coef = low_ref[pl.ds(t, systems, stride=SPAN), :]
            for s in range(b * SUB, t):
                now = now - coef[:, s : s + 1] * solved[s - b * SUB]
            solved.append(now)
            x_ref[pl.ds(t, systems, stride=SPAN), :] = now
    prefix = [None] * pairs
    for n in range(spans):
        rows = slice(n * SPAN, (n + 1) * SPAN)
        c_tail, k_tail, end = kept[n]
        for p in range(pairs):
            lanes = slice(p * LANES, (p + 1) * LANES)
            value = v_ref[rows, lanes].astype(F32)
            stacked = jnp.concatenate([c_tail[:, lanes], k_tail[:, lanes]], axis=0)
            out = []
            steps = []
            for q in range(2):
                h = 2 * p + q
                x = x_ref[(n * heads + h) * SPAN : (n * heads + h + 1) * SPAN, :]
                base, coef = reads[n * heads + h]
                out.append(base - dot_exact(coef, x, NN))
                own = jnp.where(first, value if q == 0 else pltpu.roll(value, HEAD, 1), 0.0)
                steps.append(dot_exact(jnp.concatenate([-x, own], axis=0), stacked, TN))
            local_ref[rows, lanes] = jnp.where(first, out[0], pltpu.roll(out[1], HEAD, 1))
            start_ref[rows, lanes] = jnp.where(first, pltpu.roll(out[0], HEAD, 1), out[1])
            wide = iota((2 * HEAD, LANES), 1)
            step = jnp.where(wide < HEAD, steps[0], steps[1])
            keep = jnp.exp(end[:, lanes])
            step = step + jnp.where(wide % HEAD + HEAD == iota((2 * HEAD, LANES), 0), keep, 0.0)
            prefix[p] = step if n == 0 else follow(prefix[p], step)
            if n < spans - 1:
                prefix_ref[p, n] = prefix[p]
            else:
                total_ref[p] = prefix[p].astype(total_ref.dtype)


def state_pieces(r, k, v, d, b):
    tokens, width = k.shape
    heads, spans = width // HEAD, tokens // SPAN
    pairs = heads // 2
    return pl.pallas_call(
        state_kernel,
        out_shape=(
            jax.ShapeDtypeStruct((tokens, width), F32),
            jax.ShapeDtypeStruct((tokens, width), F32),
            jax.ShapeDtypeStruct((pairs, spans - 1, 2 * HEAD, LANES), F32),
            jax.ShapeDtypeStruct((pairs, 2 * HEAD, LANES), BF16),
        ),
        scratch_shapes=[
            pltpu.VMEM((heads * tokens, LANES), F32),
            pltpu.VMEM((heads * tokens, LANES), F32),
        ],
    )(r, k, v, d, b)


def read_kernel(local_ref, start_ref, prefix_ref, in_ref, g_ref, gain_ref, out_ref):
    tokens, width = local_ref.shape
    spans = tokens // SPAN
    for n in range(spans):
        rows = slice(n * SPAN, (n + 1) * SPAN)
        tiles = []
        for p in range(width // LANES):
            lanes = slice(p * LANES, (p + 1) * LANES)
            state = in_ref[p].astype(F32)
            if n > 0:
                before = prefix_ref[p, n - 1]
                state = dot_exact(state, paired_diag(before[HEAD:]), NN) + before[:HEAD]
            tiles.append(local_ref[rows, lanes] + dot_exact(start_ref[rows, lanes], paired_diag(state), NT))
        read = jnp.concatenate(tiles, axis=1)
        centred = read - head_sums(read) * (1.0 / HEAD)
        spread = head_sums(centred * centred) * (1.0 / HEAD)
        scaled = centred * lax.rsqrt(spread + EPS_GROUP)
        gate = jax.nn.sigmoid(g_ref[rows, :].astype(F32))
        out_ref[rows, :] = (scaled * gain_ref[...] * gate).astype(out_ref.dtype)


def mixed_rows(local, start, prefix, incoming, gate_logits, gain):
    return pl.pallas_call(
        read_kernel,
        out_shape=jax.ShapeDtypeStruct(local.shape, BF16),
    )(local, start, prefix, incoming, gate_logits, gain)


def carried_in(shard, axes):
    before, so_far = None, shard
    for axis in reversed(axes):
        size, mine = lax.axis_size(axis), lax.axis_index(axis)
        pieces = lax.all_gather(so_far.astype(BF16), axis)
        inside, total = combine(pieces, mine)
        before = inside if before is None else join(inside, before)
        so_far = total
    return before[:, :HEAD]


def combine_kernel(mine_ref, pieces_ref, inside_ref, total_ref):
    size, pairs = pieces_ref.shape[0], pieces_ref.shape[1]
    mine = mine_ref[0]
    for p in range(pairs):
        so_far = pieces_ref[0, p].astype(F32)
        first = iota((2 * HEAD, LANES), 1) % HEAD + HEAD == iota((2 * HEAD, LANES), 0)
        inside = jnp.where(mine > 0, so_far, first.astype(F32))
        for n in range(1, size):
            so_far = follow(so_far, pieces_ref[n, p].astype(F32))
            inside = jnp.where(mine > n, so_far, inside)
        inside_ref[p] = inside
        total_ref[p] = so_far


def combine(pieces, mine):
    shape = jax.ShapeDtypeStruct(pieces.shape[1:], F32)
    return pl.pallas_call(
        combine_kernel,
        in_specs=[pl.BlockSpec(memory_space=pltpu.SMEM), pl.BlockSpec(memory_space=pltpu.VMEM)],
        out_shape=(shape, shape),
    )(mine.reshape(1).astype(jnp.int32), pieces)


def join_kernel(earlier_ref, later_ref, out_ref):
    for p in range(out_ref.shape[0]):
        out_ref[p] = follow(earlier_ref[p], later_ref[p])


def join(earlier, later):
    return pl.pallas_call(join_kernel, out_shape=jax.ShapeDtypeStruct(later.shape, F32))(earlier, later)


def time_mix(receptance, key_vectors, value_vectors, decay_logits, rate_logits, gate_logits, group_gain):
    read_local, start_rows, prefix, total = state_pieces(
        receptance, key_vectors, value_vectors, decay_logits, rate_logits
    )
    incoming = carried_in(total, SP)
    return mixed_rows(read_local, start_rows, prefix, incoming, gate_logits, group_gain[None, :])


def from_everyone(shard, axis):
    size = lax.axis_size(axis)
    return lax.all_to_all(
        jnp.broadcast_to(shard[None], (size, *shard.shape)), axis, 0, 0, tiled=True
    )


def joined_along(pieces, dim):
    dims = list(pieces.shape[1:])
    dims[dim] *= pieces.shape[0]
    return jnp.moveaxis(pieces, 0, dim).reshape(dims)


def gather_directly(shard, axis, dim):
    pieces = from_everyone(shard, axis)
    return joined_along(pieces, dim)


def of_everyone(shard, axis):
    everything = from_everyone(shard, axis)
    return jnp.sum(everything, axis=0)


def split_up(shard, dim, size):
    before, after = (shard.shape[:dim], shard.shape[dim + 1 :])
    return jnp.moveaxis(shard.reshape(*before, size, -1, *after), dim, 0)


def sent_and_summed(shard, axis, dim):
    size = lax.axis_size(axis)
    pieces = lax.all_to_all(split_up(shard, dim, size), axis, 0, 0, tiled=True)
    return jnp.sum(pieces.astype(jnp.float32), axis=0)


def local(
    receptance,
    key_vectors,
    value_vectors,
    decay_logits,
    rate_logits,
    gate_logits,
    group_gain,
    residual,
    mixer_out,
    norm_gain,
    expert_ids,
    route_weight,
    expert_gate,
    expert_up,
    expert_down,
):
    mixed_rows = time_mix(
        receptance, key_vectors, value_vectors, decay_logits, rate_logits, gate_logits, group_gain
    )
    tokens_here, features = residual.shape
    projected = jnp.dot(
        gather_directly(mixed_rows, "tp", 1), mixer_out, preferred_element_type=jnp.float32
    )
    midway = (residual.astype(jnp.float32) + projected).astype(jnp.bfloat16)
    midway_f = midway.astype(jnp.float32)
    squares = of_everyone(jnp.sum(midway_f * midway_f, axis=1), "tp")
    inv_rms = lax.rsqrt(squares / D + EPS_NORM)
    normed = (midway_f * norm_gain[None, :] * inv_rms[:, None]).astype(jnp.bfloat16)
    routes = expert_ids.shape[1]
    experts_all = lax.axis_size(SP) * expert_gate.shape[0]
    capacity = 2 * tokens_here * routes // experts_all
    flat_ids = expert_ids.reshape(-1)
    onehot = (flat_ids[:, None] == jnp.arange(experts_all, dtype=jnp.int32)[None, :]).astype(
        jnp.int32
    )
    earlier_count = jnp.sum((jnp.cumsum(onehot, axis=0) - onehot) * onehot, axis=1)
    slot_of = flat_ids * capacity + earlier_count
    owner_token = jnp.arange(tokens_here * routes, dtype=jnp.int32) // routes
    slot_table = (
        jnp.full((experts_all * capacity,), tokens_here, jnp.int32).at[slot_of].set(owner_token)
    )
    padded = jnp.concatenate([normed, jnp.zeros((1, features), jnp.bfloat16)], axis=0)
    outgoing = padded[slot_table].reshape(experts_all, capacity, features)
    arrived = lax.all_to_all(outgoing, SP, split_axis=0, concat_axis=0, tiled=True)
    arrived_rows = arrived.reshape(-1, features)
    paired = jnp.concatenate([expert_gate[0], expert_up[0]], axis=1)
    gate_up = sent_and_summed(
        jnp.dot(arrived_rows, paired, preferred_element_type=jnp.float32).astype(jnp.bfloat16),
        "tp",
        0,
    )
    half_width = paired.shape[1] // 2
    hidden = (jax.nn.silu(gate_up[:, :half_width]) * gate_up[:, half_width:]).astype(jnp.bfloat16)
    expert_res = jnp.dot(
        gather_directly(hidden, "tp", 0), expert_down[0], preferred_element_type=jnp.float32
    )
    returned = lax.all_to_all(
        expert_res.astype(jnp.bfloat16).reshape(-1, capacity, features),
        SP,
        split_axis=0,
        concat_axis=0,
        tiled=True,
    )
    picked = (
        returned.reshape(-1, features)[slot_of]
        .astype(jnp.float32)
        .reshape(tokens_here, routes, features)
    )
    routed_sum = jnp.sum(picked * route_weight[:, :, None], axis=1)
    return (midway_f + routed_sum).astype(jnp.bfloat16)


def solution(mesh):
    torus = Mesh(mesh.devices.reshape(16, 2, mesh.shape["tp"]), ("sp_0", "sp_1", "tp"))
    return jax.shard_map(
        local,
        mesh=torus,
        in_specs=(
            P(SP, "tp"),
            P(SP, "tp"),
            P(SP, "tp"),
            P(SP, "tp"),
            P(SP, "tp"),
            P(SP, "tp"),
            P("tp"),
            P(SP, "tp"),
            P(None, "tp"),
            P("tp"),
            P(SP, None),
            P(SP, None),
            P(SP, "tp", None),
            P(SP, "tp", None),
            P(SP, None, "tp"),
        ),
        out_specs=P(SP, "tp"),
        check_vma=False,
    )
```

time: 453 us -> 344 us (0.76)
  other arithmetic: 96.4 us -> 5.25 us
  waiting for transfers between devices: 55.2 us -> 117 us
  blocking collectives: 206 us -> 145 us
  matrix products: 46.5 us -> 6.24 us
  Pallas kernels: 0 us -> 23.6 us
  local copies, waits for them, and re-layouts: 30.4 us -> 14.7 us
  between operations: 0.89 us -> 13.6 us
    another operation x8 -> x2, other arithmetic: 82.5 us -> 1.2 us  [the longest x3 80.9 us: block_pieces(): jax.scipy.linalg.solve_triangular(system, jnp.concatenate([right_local, r...]
    all_gather x0 -> x1, waiting for transfers between devices: none -> 59.1 us  [carried_in(): pieces = lax.all_gather(so_far.astype(BF16), axis)]
    all_gather x4 -> x1, blocking collectives: 65.9 us -> 10 us  [carried_in(): pieces = lax.all_gather(so_far.astype(BF16), axis)]
    dot_general x53 -> x0, matrix products: 39.1 us -> none  [exact_einsum(): return jnp.einsum(pattern, first_op, second_op, precision=HIGHEST)]
    pallas_call x0 -> x5, Pallas kernels: none -> 23.6 us  [the longest x1 9.63 us: state_pieces(): pl.pallas_call(state_kernel, out_shape=(jax.ShapeDtypeStruct((tokens, wid...]
    dynamic_update_slice x8 -> x0, local copies, waits for them, and re-layouts: 5.47 us -> none  [time_mix(): lax.scan(advance, (zero_heads, eye_heads), (block_map, block_add))]
    dynamic_update_slice x8 -> x0, other arithmetic: 5.32 us -> none  [time_mix(): lax.scan(advance, (zero_heads, eye_heads), (block_map, block_add))]
    all_to_all x1, blocking collectives: 56.7 us -> 51.9 us  [local(): lax.all_to_all(outgoing, SP, split_axis=0, concat_axis=0, tiled=True)]
  transfers between devices with their start and end apart: 3 -> 4, of which waited for: 3 -> 4; matrix products, arithmetic and copies ran while one was open for 1% -> 1% of each run, Pallas kernels for 0% -> 0%
where the time goes in v1:
time: 344 us
  blocking collectives  145 us (42%)
  waiting for transfers between devices  117 us (34%)
  Pallas kernels  23.6 us (7%)
  starting transfers between devices  18.3 us (5%)
  local copies, waits for them, and re-layouts  14.7 us (4%)
  between operations  13.6 us (4%)
  matrix products  6.24 us (2%)
  other arithmetic  5.25 us (2%)
    all_gather x1, waiting for transfers between devices, carried_in(): pieces = lax.all_gather(so_far.astype(BF16), axis)  59.1 us
    all_to_all x1, blocking collectives, sent_and_summed(): pieces = lax.all_to_all(split_up(shard, dim, size), axis, 0, 0, tiled=True)  52.7 us
    all_to_all x1, blocking collectives, local(): lax.all_to_all(outgoing, SP, split_axis=0, concat_axis=0, tiled=True)  51.9 us
    all_to_all x1, waiting for transfers between devices, local(): lax.all_to_all(expert_res.astype(jnp.bfloat16).reshape(-1, capacity, feat...  33.4 us
    all_to_all x1, blocking collectives, from_everyone(): lax.all_to_all(jnp.broadcast_to(shard[None], (size, *shard.shape)), axis,...  30.5 us
    all_to_all x2, waiting for transfers between devices, from_everyone(): lax.all_to_all(jnp.broadcast_to(shard[None], (size, *shard.shape)), axis,...  24.2 us
    all_to_all x2, starting transfers between devices, from_everyone(): lax.all_to_all(jnp.broadcast_to(shard[None], (size, *shard.shape)), axis,...  11.1 us
    all_gather x1, blocking collectives, carried_in(): pieces = lax.all_gather(so_far.astype(BF16), axis)  10 us
  transfers between devices with their start and end apart: 4, of which 4 were waited for; matrix products, arithmetic and copies ran while one was open for 1% of the time, Pallas kernels for 0%

profile of v1, /device:TPU:1, one launch (start us, length us, event | category | flops | bytes accessed | tf_op | source)
XLA Modules:
  0.0 343.7 jit_solution(14735269733109792067)
XLA Ops:
  6.5 0.0 copy-start
  6.5 0.0 all-gather.4.cloned.1.call-start
  6.5 9.6 %shard_map.145 = (f32[256,256]{1,0:T(8,128)}, f32[256,256]{1,0:T(8,128)}, f32[2,3,128,128]{3,2,1,0:T(8,128)}, bf16[2,128,128]{2,1,0:T(8,128)(2,1)}) custom-call(bf16[256,256]{1,0:T(8,128)(2,1)} %r_ref.1, bf16[256,256]{1,0:T(8,128)(2,1)} %k_ref.1, bf16[256,256]{1,0:T(8,128)(2,1)} %v_ref.1, bf16[256,256]{1,0:T(8,128)(2,1)} %d_ref.1, bf16[256,256]{1,0:T(8,128)(2,1)} %b_ref.1), custom_call_target="tpu_custom_call" | custom-call | tf_op jit(solution)/shard_map/pallas_call | solution.py:180
  16.2 10.0 %all-gather = bf16[4,128,128]{2,1,0:T(8,128)(2,1)} all-gather(bf16[2,128,128]{2,1,0:T(8,128)(2,1)} %get-tuple-element.15), channel_id=2, replica_groups=mesh['sp_0'=16,'sp_1'=2,'tp'=16] {'sp_1'}, dimensions={0}, use_global_device_ids=true | all-gather | bytes 196608 | tf_op jit(solution)/shard_map/all_gather | solution.py:227
  26.2 1.8 shard_map.146
  28.0 1.5 convert_element_type.45
  29.5 0.0 all-gather.4.cloned.1.call-update
  29.6 59.1 %all-gather.4.cloned.1.call-done = bf16[32,128,128]{2,1,0:T(8,128)(2,1)} async-done(((bf16[2,128,128]{2,1,0:T(8,128)(2,1)}), bf16[32,128,128]{2,1,0:T(8,128)(2,1)}) %all-gather.4.cloned.1.call-update) | async-done | bytes 1048592 | tf_op jit(solution)/shard_map/all_gather | solution.py:227
  88.7 6.4 %shard_map.147 = (f32[2,128,128]{2,1,0:T(8,128)}, f32[2,128,128]{2,1,0:T(8,128)}) custom-call(s32[1]{0:T(128)} %bitcast.mine_ref, bf16[16,2,128,128]{3,2,1,0:T(8,128)(2,1)} %bitcast.49), custom_call_target="tpu_custom_call" | custom-call | tf_op jit(solution)/shard_map/pallas_call | solution.py:250
  95.1 1.8 shard_map.148
  96.9 1.5 slice.24.in_ref
  98.3 4.0 %shard_map.149 = bf16[256,256]{1,0:T(8,128)(2,1)} custom-call(f32[256,256]{1,0:T(8,128)} %get-tuple-element.12.local_ref, f32[256,256]{1,0:T(8,128)} %get-tuple-element.13.start_ref, f32[2,3,128,128]{3,2,1,0:T(8,128)} %get-tuple-element.14.prefix_ref, f32[2,64,128]{2,1,0:T(8,128)} %slice.24.in_ref, bf16[256,256]{1,0:T(8,128)(2,1)} %g_ref.1, f32[1,256]{1,0:T(1,128)} %bitcast.56), custom_call_target="tpu_custom_call" | custom-call | tf_op jit(solution)/shard_map/pallas_call | solution.py:217
  102.3 1.0 copy.35
  103.3 1.5 broadcast_in_dim.13
  104.8 0.0 copy-start.2
  104.8 0.0 copy-start.6
  104.8 6.7 %all-to-all-start = ((bf16[16,256,256]{1,2,0:T(8,128)(2,1)}), bf16[16,256,256]{1,2,0:T(8,128)(2,1)}, u32[]{:S(2)}, u32[]{:S(2)}) async-start(bf16[16,256,256]{1,2,0:T(8,128)(2,1)} %broadcast_in_dim.13), calls=%async_computation | async-start | bytes 4194304 | tf_op jit(solution)/shard_map/all_to_all | solution.py:276
  111.6 0.0 copy-done.2
  111.6 0.1 copy.38
  111.7 0.1 eq.29
  111.9 0.1 eq.25
  112.0 1.2 reduce-window.6
  113.2 0.2 slice_reduce_fusion
  113.5 0.1 copy.37
  113.6 0.1 mul.60
  113.8 0.1 fusion.9
  113.9 2.6 scatter_custom_fusion
  116.5 17.8 %all-to-all-done = bf16[16,256,256]{1,2,0:T(8,128)(2,1)} async-done(((bf16[16,256,256]{1,2,0:T(8,128)(2,1)}), bf16[16,256,256]{1,2,0:T(8,128)(2,1)}, u32[]{:S(2)}, u32[]{:S(2)}) %all-to-all-start) | async-done | bytes 2097184 | tf_op jit(solution)/shard_map/all_to_all | solution.py:276
  134.3 0.0 copy-done
  134.3 0.0 copy-done.6
  134.3 0.0 copy-start.4
  134.3 2.4 multiply_reduce_fusion.1
  136.8 0.6 broadcast_in_dim.14
  137.4 4.4 %all-to-all-start.1 = ((f32[16,1,256]{2,1,0:T(1,128)}), f32[16,1,256]{2,1,0:T(1,128)S(1)}, u32[]{:S(2)}, u32[]{:S(2)}) async-start(f32[16,1,256]{2,1,0:T(1,128)} %broadcast_in_dim.14), calls=%async_computation.1 | async-start | bytes 32768 | tf_op jit(solution)/shard_map/all_to_all | solution.py:276
  141.8 6.4 %all-to-all-done.1 = f32[16,1,256]{2,1,0:T(1,128)S(1)} async-done(((f32[16,1,256]{2,1,0:T(1,128)}), f32[16,1,256]{2,1,0:T(1,128)S(1)}, u32[]{:S(2)}, u32[]{:S(2)}) %all-to-all-start.1) | async-done | bytes 16416 | tf_op jit(solution)/shard_map/all_to_all | solution.py:276
  148.3 0.0 copy-done.4
  148.3 0.1 multiply_convert_fusion
  148.4 0.0 copy-start.1
  148.4 3.9 %gather_fusion = bf16[1024,256]{1,0:T(8,128)(2,1)S(1)} fusion(bf16[257,256]{1,0:T(8,128)(2,1)S(1)} %concatenate.6, s32[1024]{0:T(1024)S(1)} %fusion.11), kind=kCustom, calls=%fused_computation | custom fusion | bytes 1052672 | tf_op jit(solution)/shard_map/gather | solution.py:351
  152.4 51.9 %all_to_all.31 = bf16[32,32,256]{2,1,0:T(8,128)(2,1)S(1)} all-to-all(bf16[32,32,256]{2,1,0:T(8,128)(2,1)S(1)} %bitcast.48), channel_id=1, replica_groups=mesh['sp_0'=16,'sp_1'=2,'tp'=16] {'sp_0','sp_1'}, dimensions={0} | all-to-all | bytes 1048576 | tf_op jit(solution)/shard_map/all_to_all | solution.py:352
  204.3 0.0 copy-done.1
  204.3 2.3 convolution_convert_fusion
  206.6 52.7 %all_to_all.32 = bf16[16,64,2048]{2,1,0:T(8,128)(2,1)S(1)} all-to-all(bf16[16,64,2048]{2,1,0:T(8,128)(2,1)S(1)} %bitcast.44), channel_id=1, replica_groups=mesh['sp_0'=16,'sp_1'=2,'tp'=16] {'tp'}, dimensions={0} | all-to-all | bytes 8388608 | tf_op jit(solution)/shard_map/all_to_all | solution.py:304
  259.3 0.8 convert_reduce_fusion
  260.1 0.1 fusion.6
  260.2 0.3 broadcast_in_dim.17
  260.4 0.0 copy-start.5
  260.4 30.5 %all_to_all.33 = bf16[16,64,1024]{2,1,0:T(8,128)(2,1)S(1)} all-to-all(bf16[16,64,1024]{2,1,0:T(8,128)(2,1)S(1)} %broadcast_in_dim.17), channel_id=1, replica_groups=mesh['sp_0'=16,'sp_1'=2,'tp'=16] {'tp'}, dimensions={0} | all-to-all | bytes 4194304 | tf_op jit(solution)/shard_map/all_to_all | solution.py:276
  291.0 0.0 copy-done.5
  291.0 0.0 copy-start.3
  291.0 1.5 convolution_convert_fusion.1
  292.5 7.2 %all-to-all-start.5 = ((bf16[32,32,256]{2,1,0:T(8,128)(2,1)}), bf16[32,32,256]{2,1,0:T(8,128)(2,1)S(1)}, u32[]{:S(2)}, u32[]{:S(2)}) async-start(bf16[32,32,256]{2,1,0:T(8,128)(2,1)} %bitcast.17), calls=%async_computation.5 | async-start | bytes 1048576 | tf_op jit(solution)/shard_map/all_to_all | solution.py:365
  299.7 0.0 copy-done.3
  299.7 0.1 copy.41
  299.9 33.4 %all-to-all-done.5 = bf16[32,32,256]{2,1,0:T(8,128)(2,1)S(1)} async-done(((bf16[32,32,256]{2,1,0:T(8,128)(2,1)}), bf16[32,32,256]{2,1,0:T(8,128)(2,1)S(1)}, u32[]{:S(2)}, u32[]{:S(2)}) %all-to-all-start.5) | async-done | bytes 524320 | tf_op jit(solution)/shard_map/all_to_all | solution.py:365
  333.2 1.9 gather_fusion.1
  335.2 0.3 reshape.102
  335.5 0.7 multiply_reduce_fusion
  336.2 0.7 add_convert_fusion
  (11 shorter events, 0.1 us)
Async XLA Ops:
  6.5 127.8 %copy-start = (bf16[4096,256]{1,0:T(8,128)(2,1)S(1)}, bf16[4096,256]{1,0:T(8,128)(2,1)}, u32[]{:S(2)}) copy-start(bf16[4096,256]{1,0:T(8,128)(2,1)} %param.23) | copy-start | bytes 6291460
  6.5 82.1 %all-gather.4.cloned.1.call-start = ((), (), s32[]{:S(2)}) async-start(), calls=%async_computation.6 | async-start | bytes 1114112 | tf_op jit(solution)/shard_map/all_gather | solution.py:227
  104.8 6.7 %copy-start.2 = (s32[256,2]{0,1:T(2,128)S(1)}, s32[256,2]{0,1:T(2,128)}, u32[]{:S(2)}) copy-start(s32[256,2]{0,1:T(2,128)} %param.25) | copy-start | bytes 6148
  104.8 29.5 %copy-start.6 = (bf16[256,256]{1,0:T(8,128)(2,1)S(1)}, bf16[256,256]{1,0:T(8,128)(2,1)}, u32[]{:S(2)}) copy-start(bf16[256,256]{1,0:T(8,128)(2,1)} %param.22) | copy-start | bytes 393220
  104.8 29.5 %all-to-all-start = ((bf16[16,256,256]{1,2,0:T(8,128)(2,1)}), bf16[16,256,256]{1,2,0:T(8,128)(2,1)}, u32[]{:S(2)}, u32[]{:S(2)}) async-start(bf16[16,256,256]{1,2,0:T(8,128)(2,1)} %broadcast_in_dim.13), calls=%async_computation | async-start | bytes 4194304 | tf_op jit(solution)/shard_map/all_to_all | solution.py:276
  134.3 14.0 %copy-start.4 = (f32[256]{0:T(256)S(1)}, f32[256]{0:T(256)}, u32[]{:S(2)}) copy-start(f32[256]{0:T(256)} %param.24) | copy-start | bytes 3076
  137.4 10.9 %all-to-all-start.1 = ((f32[16,1,256]{2,1,0:T(1,128)}), f32[16,1,256]{2,1,0:T(1,128)S(1)}, u32[]{:S(2)}, u32[]{:S(2)}) async-start(f32[16,1,256]{2,1,0:T(1,128)} %broadcast_in_dim.14), calls=%async_computation.1 | async-start | bytes 32768 | tf_op jit(solution)/shard_map/all_to_all | solution.py:276
  148.4 55.9 %copy-start.1 = (bf16[1,256,1024]{2,1,0:T(8,128)(2,1)S(1)}, bf16[1,256,1024]{2,1,0:T(8,128)(2,1)}, u32[]{:S(2)}) copy-start(bf16[1,256,1024]{2,1,0:T(8,128)(2,1)} %param.28) | copy-start | bytes 1572868
  260.4 30.5 %copy-start.5 = (bf16[1,1024,256]{2,1,0:T(8,128)(2,1)S(1)}, bf16[1,1024,256]{2,1,0:T(8,128)(2,1)}, u32[]{:S(2)}) copy-start(bf16[1,1024,256]{2,1,0:T(8,128)(2,1)} %param.29) | copy-start | bytes 1572868
  291.0 8.8 %copy-start.3 = (f32[256,2]{0,1:T(2,128)S(1)}, f32[256,2]{0,1:T(2,128)}, u32[]{:S(2)}) copy-start(f32[256,2]{0,1:T(2,128)} %param.26) | copy-start | bytes 6148
  292.5 40.8 %all-to-all-start.5 = ((bf16[32,32,256]{2,1,0:T(8,128)(2,1)}), bf16[32,32,256]{2,1,0:T(8,128)(2,1)S(1)}, u32[]{:S(2)}, u32[]{:S(2)}) async-start(bf16[32,32,256]{2,1,0:T(8,128)(2,1)} %bitcast.17), calls=%async_computation.5 | async-start | bytes 1048576 | tf_op jit(solution)/shard_map/all_to_all | solution.py:365
Sparse Core Ops, SparseCore 0:
  29.7 58.9 all-gather.3
